TPU v7x, 32 devices: a whole 2x2x4 slice. The times are simulated.
32 devices in a mesh: rep: 2 (over x), fs: 4 (over z), tp: 4 (over y, core).
Axes of the slice: x: 2, y: 2, z: 4, core: 2. Of those that a mesh axis runs over, the one named last changes fastest.
Arguments:
- tokens: bfloat16 [4096, 1024], P(('rep', 'fs', 'tp')), may hold values from -6 to 6
- w_up: bfloat16 [1024, 4096], P('fs', 'tp'), may hold values from -0.1875 to 0.1875
- w_down: bfloat16 [4096, 1024], P('tp', 'fs'), may hold values from -0.09375 to 0.09375
- out_gain: float32 [1024], replicated, may hold values from 0.1 to 1.9
- out_shift: float32 [1024], replicated, may hold values from -3 to 3
Outputs:
- normed: bfloat16 [4096, 1024], P(('rep', 'fs', 'tp'))
All inputs are finite; a program needn't handle non-finite values.
Results may differ from a plain program's by a relative error of at most 0.015.
Values may be sent and summed in bfloat16 or wider, within the bound.
A program may use at most 64 MiB of HBM per device.

v0:
```python
import jax
import jax.numpy as jnp
from jax import lax
from jax.sharding import PartitionSpec as P

residual_scale = 2.0**0.25
norm_eps = 1e-05


def over_all(share, axis, dim, apply):
    everything = lax.all_gather(share, axis, axis=dim, tiled=True)
    return apply(everything, jnp.int32(0))


def summed_rows(product, extent, axis):
    whole = product(jnp.int32(0), extent * lax.axis_size(axis)).astype(jnp.bfloat16)
    return lax.psum_scatter(whole, axis, scatter_dimension=0, tiled=True).astype(jnp.float32)


def layer_norm(summed, out_gain, out_shift):
    row_mean = jnp.mean(summed, axis=-1, keepdims=True)
    centered = summed - row_mean
    row_var = jnp.mean(centered * centered, axis=-1, keepdims=True)
    return centered * lax.rsqrt(row_var + norm_eps) * out_gain + out_shift


def squared_relu(pre_act):
    return jnp.square(jnp.maximum(pre_act, 0.0)).astype(jnp.bfloat16)


def shards(tokens, w_up, w_down, out_gain, out_shift):
    up_block = lax.all_gather(w_up, "fs", axis=0, tiled=True)

    def activate(block_rows, offset):
        return squared_relu(jnp.dot(block_rows, up_block, preferred_element_type=jnp.float32))

    hidden = over_all(tokens, "tp", 0, activate)
    down_block = lax.all_gather(w_down, "fs", axis=1, tiled=True)
    own_count = tokens.shape[0]

    def project(offset, how_many):
        picked = lax.dynamic_slice_in_dim(hidden, offset, how_many, 0)
        return jnp.dot(picked, down_block, preferred_element_type=jnp.float32)

    branch = summed_rows(project, own_count, "tp")
    summed = residual_scale * tokens.astype(jnp.float32) + branch
    return layer_norm(summed, out_gain, out_shift).astype(jnp.bfloat16)


def solution(mesh):
    in_specs = (P(("rep", "fs", "tp"), None), P("fs", "tp"), P("tp", "fs"), P(), P())
    out_specs = P(("rep", "fs", "tp"), None)
    return jax.shard_map(shards, mesh=mesh, in_specs=in_specs, out_specs=out_specs, check_vma=False)
```

profile of v0, /device:TPU:0, one launch (start us, length us, event | category | flops | bytes accessed | tf_op | source)
XLA Modules:
  0.0 163.1 jit_solution(3515093248988575749)
XLA Ops:
  6.5 0.0 all-gather.4.cloned.1.call-start
  6.5 0.7 all-gather.4.cloned.1.call-update
  7.3 0.0 all-gather.6.cloned.1.call-start
  7.3 0.7 all-gather.6.cloned.1.call-update
  8.0 0.0 all-gather.8.cloned.1.call-start
  8.1 0.7 all-gather.8.cloned.1.call-update
  8.7 0.0 copy-start
  8.8 0.0 reduce-scatter.2.cloned.1.call-start
  8.8 19.5 %all-gather.4.cloned.1.call-done = bf16[512,1024]{1,0:T(8,128)(2,1)} async-done(((bf16[128,1024]{1,0:T(8,128)(2,1)}), bf16[512,1024]{1,0:T(8,128)(2,1)}) %all-gather.4.cloned.1.call-update) | async-done | bytes 1048592 | tf_op jit(solution)/shard_map/all_gather | solution.py:11
  28.3 47.0 %all-gather.6.cloned.1.call-done = bf16[1024,1024]{1,0:T(8,128)(2,1)} async-done(((bf16[256,1024]{1,0:T(8,128)(2,1)}), bf16[1024,1024]{1,0:T(8,128)(2,1)}) %all-gather.6.cloned.1.call-update) | async-done | bytes 2097168 | tf_op jit(solution)/shard_map/all_gather | solution.py:32
  75.3 47.9 %all-gather.8.cloned.1.call-done = bf16[1024,1024]{1,0:T(8,128)(2,1)} async-done(((bf16[1024,256]{1,0:T(8,128)(2,1)}), bf16[1024,1024]{1,0:T(8,128)(2,1)}) %all-gather.8.cloned.1.call-update) | async-done | bytes 2097168 | tf_op jit(solution)/shard_map/all_gather | solution.py:38
  123.2 5.8 %convolution_convert_fusion = bf16[512,1024]{1,0:T(8,128)(2,1)} fusion(bf16[1024,1024]{1,0:T(8,128)(2,1)} %all-gather.8.cloned.1.call-done, bf16[512,1024]{1,0:T(8,128)(2,1)} %all-gather.4.cloned.1.call-done, bf16[1024,1024]{1,0:T(8,128)(2,1)} %all-gather.6.cloned.1.call-done), kind=kOutput, calls=%fused_computation.1 | convolution fusion | flops 2149580800 | bytes 6291456 | tf_op jit(solution)/shard_map/dot_general | solution.py:43
  129.1 0.0 copy-start.1
  129.1 0.0 copy-start.2
  129.1 0.0 reduce-scatter.2.cloned.1.call-update
  129.1 23.3 %reduce-scatter.2.cloned.1.call-done = bf16[128,1024]{1,0:T(8,128)(2,1)} async-done(((bf16[512,1024]{1,0:T(8,128)(2,1)}), bf16[128,1024]{1,0:T(8,128)(2,1)}) %reduce-scatter.2.cloned.1.call-update) | async-done | bytes 262160 | tf_op jit(solution)/shard_map/reduce_scatter | solution.py:17
  152.5 0.0 copy-done
  152.5 1.1 fusion
  153.6 1.2 multiply_reduce_fusion
  154.7 0.0 copy-done.1
  154.7 0.0 copy-done.2
  154.8 1.8 %add_convert_fusion = bf16[128,1024]{1,0:T(8,128)(2,1)} fusion(bf16[128,1024]{1,0:T(8,128)(2,1)} %reduce-scatter.2.cloned.1.call-done, bf16[128,1024]{1,0:T(8,128)(2,1)S(1)} %copy-done, f32[1024]{0:T(1024)S(1)} %copy-done.1, f32[1024]{0:T(1024)S(1)} %copy-done.2, f32[128]{0:T(128)S(1)} %add_rsqrt_fusion, f32[128]{0:T(128)S(1)} %broadcast_multiply_fusion), kind=kLoop, calls=%fused_computation.2 | loop fusion | flops 1179648 | bytes 795648 | tf_op jit(solution)/shard_map/convert_element_type | solution.py:47
  (2 shorter events, 0.0 us)
Async XLA Ops:
  6.5 21.7 %all-gather.4.cloned.1.call-start = ((), (), s32[]{:S(2)}) async-start(), calls=%async_computation.1 | async-start | bytes 1310720 | tf_op jit(solution)/shard_map/all_gather | solution.py:11
  7.3 68.0 %all-gather.6.cloned.1.call-start = ((), (), s32[]{:S(2)}) async-start(), calls=%async_computation.2 | async-start | bytes 2621440 | tf_op jit(solution)/shard_map/all_gather | solution.py:32
  8.0 115.2 %all-gather.8.cloned.1.call-start = ((), (), s32[]{:S(2)}) async-start(), calls=%async_computation.3 | async-start | bytes 2621440 | tf_op jit(solution)/shard_map/all_gather | solution.py:38
  8.7 143.7 %copy-start = (bf16[128,1024]{1,0:T(8,128)(2,1)S(1)}, bf16[128,1024]{1,0:T(8,128)(2,1)}, u32[]{:S(2)}) copy-start(bf16[128,1024]{1,0:T(8,128)(2,1)} %param.5) | copy-start | bytes 786436
  8.8 143.7 %reduce-scatter.2.cloned.1.call-start = ((), (), s32[]{:S(2)}) async-start(), calls=%async_computation.4 | async-start | bytes 1310720 | tf_op jit(solution)/shard_map/reduce_scatter | solution.py:17
  129.1 25.7 %copy-start.1 = (f32[1024]{0:T(1024)S(1)}, f32[1024]{0:T(1024)}, u32[]{:S(2)}) copy-start(f32[1024]{0:T(1024)} %param.9) | copy-start | bytes 12292
  129.1 25.7 %copy-start.2 = (f32[1024]{0:T(1024)S(1)}, f32[1024]{0:T(1024)}, u32[]{:S(2)}) copy-start(f32[1024]{0:T(1024)} %param.8) | copy-start | bytes 12292
Sparse Core Ops, SparseCore 0:
  8.9 19.3 all-gather.3
  29.8 45.4 all-gather.5
  76.9 46.3 all-gather.7
  129.2 23.1 reduce-scatter.1
where the time goes:
time: 163 us
  waiting for transfers between devices  140 us (86%)
  between operations  13.2 us (8%)
  matrix products  5.85 us (4%)
  other arithmetic  4.1 us (3%)
    all_gather x1, waiting for transfers between devices, shards(): down_block = lax.all_gather(w_down, 'fs', axis=1, tiled=True)  47.9 us
    all_gather x1, waiting for transfers between devices, shards(): up_block = lax.all_gather(w_up, 'fs', axis=0, tiled=True)  47 us
    reduce_scatter x1, waiting for transfers between devices, summed_rows(): lax.psum_scatter(whole, axis, scatter_dimension=0, tiled=True)  23.3 us
    all_gather x1, waiting for transfers between devices, over_all(): everything = lax.all_gather(share, axis, axis=dim, tiled=True)  19.5 us
    dot_general x1, matrix products, project(): return jnp.dot(picked, down_block, preferred_element_type=jnp.float32)  5.85 us
  transfers between devices with their start and end apart: 4, of which 4 were waited for; matrix products, arithmetic and copies ran while one was open for 0% of the time, Pallas kernels for 0%

commit v1 on v0

v1 whole, which is shorter than its diff:
```python
import functools

import jax
import jax.numpy as jnp
from jax import lax
from jax.experimental import pallas as pl
from jax.experimental.pallas import tpu as pltpu
from jax.sharding import PartitionSpec as P

residual_scale = 2.0**0.25
norm_eps = 1e-05


def kernel(
    sizes,
    tokens_ref, up_ref, down_ref, gain_ref, shift_ref,
    out_ref,
    tok, up, down, hidden, s1, r1, acc, s2, r2, own2,
    load_sem, tok_send, tok_recv, fwd_send, up_send, up_recv,
    down_send, down_recv, s1_send, r1_recv, s2_send, r2_recv,
):
    R, F, T = sizes
    Y = T // 2
    pairs = R * Y
    own = tokens_ref.shape[0]
    H = up.shape[2]
    half = H // 2
    Dc = down.shape[2]
    r, f, t = lax.axis_index("rep"), lax.axis_index("fs"), lax.axis_index("tp")
    y, c = t // 2, t % 2
    q = r * Y + y
    mine = c * pairs + q

    def dev(rr, ff, tt):
        return {"rep": rr, "fs": ff, "tp": tt}

    partner = dev(r, f, y * 2 + (1 - c))
    peers = []
    for dr in range(R):
        for dy in range(Y):
            if dr or dy:
                rr, yy = (r + dr) % R, (y + dy) % Y
                sr, sy = (r + R - dr) % R, (y + Y - dy) % Y
                peers.append((dev(rr, f, yy * 2 + c), rr * Y + yy, sr * Y + sy))

    def remote(src, dst, ss, rs, device):
        return pltpu.make_async_remote_copy(
            src_ref=src, dst_ref=dst, send_sem=ss, recv_sem=rs,
            device_id=device, device_id_type=pl.DeviceIdType.MESH,
        )

    base = pl.multiple_of(r * H, H)
    loads = [
        pltpu.make_async_copy(up_ref.at[:, pl.ds(base, H)], up.at[f], load_sem.at[0]),
        pltpu.make_async_copy(tokens_ref, tok.at[mine], load_sem.at[1]),
        pltpu.make_async_copy(down_ref.at[pl.ds(base, H), :], down.at[f], load_sem.at[2]),
    ]
    for load in loads:
        load.start()

    barrier = pltpu.get_barrier_semaphore()

    def greet(device):
        pl.semaphore_signal(barrier, inc=1, device_id=device, device_id_type=pl.DeviceIdType.MESH)

    greet(partner)
    for device, _, _ in peers:
        greet(device)

    @pl.when(f > 0)
    def _():
        greet(dev(r, f - 1, t))

    @pl.when(f < F - 1)
    def _():
        greet(dev(r, f + 1, t))

    neighbours = jnp.where(f > 0, 1, 0) + jnp.where(f < F - 1, 1, 0)
    pl.semaphore_wait(barrier, 1 + len(peers) + neighbours)

    def up_copy(piece, to, n):
        return remote(up.at[piece], up.at[piece], up_send.at[n], up_recv.at[piece], dev(r, to, t))

    def down_copy(piece, part, to, n):
        block = down.at[piece, pl.ds(part * half, half)]
        return remote(block, block, down_send.at[n, part], down_recv.at[piece, part], dev(r, to, t))

    def guarded(condition, action):
        @pl.when(condition)
        def _():
            action()

    last = 2 * F - 2

    def own_sends(copy):
        guarded(f < F - 1, lambda: copy(f + 1, last + 1).start())
        guarded(f > 0, lambda: copy(f - 1, 0).start())

    loads[0].wait()
    own_sends(lambda to, n: up_copy(f, to, n))
    loads[1].wait()
    tok_copies = [remote(tok.at[mine], tok.at[mine], tok_send.at[0], tok_recv.at[mine], partner)]
    for k, (device, _, _) in enumerate(peers):
        tok_copies.append(remote(tok.at[mine], tok.at[mine], tok_send.at[k + 1], tok_recv.at[mine], device))
    for copy in tok_copies[1:] + tok_copies[:1]:
        copy.start()
    loads[2].wait()
    own_sends(lambda to, n: down_copy(f, 0, to, n))

    def up_visit(v):
        s = (v - 1) // 2
        if v % 2:
            piece, to = f - 1 - s, f + 1
            here, onward = piece >= 0, jnp.logical_and(piece >= 0, f < F - 1)
        else:
            piece, to = f + 1 + s, f - 1
            here, onward = piece < F, jnp.logical_and(piece < F, f > 0)
        return piece, to, here, onward

    def take_up(v):
        piece, to, here, onward = up_visit(v)
        guarded(here, lambda: up_copy(piece, f, v).wait_recv())
        guarded(onward, lambda: up_copy(piece, to, v).start())

    for v in (1, 2):
        if v <= last:
            take_up(v)
    own_sends(lambda to, n: down_copy(f, 1, to, n))

    fwd_copies = []
    for k, (_, _, source) in enumerate(peers):
        slot = c * pairs + source
        remote(tok.at[slot], tok.at[slot], tok_send.at[0], tok_recv.at[slot], partner).wait_recv()
        fwd = remote(tok.at[slot], tok.at[slot], fwd_send.at[k], tok_recv.at[slot], partner)
        fwd.start()
        fwd_copies.append(fwd)

    for v in range(3, last + 1):
        take_up(v)
    for k in range(pairs):
        slot = (1 - c) * pairs + k
        remote(tok.at[slot], tok.at[slot], tok_send.at[0], tok_recv.at[slot], partner).wait_recv()

    rows = pairs * own
    chunk = 2 if pairs % 2 == 0 else 1
    weights = lambda: up[...].reshape(up.shape[0] * up.shape[1], H)

    @pl.loop(0, 2 * pairs // chunk)
    def _(n):
        block = tok[pl.ds(n * chunk, chunk)].reshape(chunk * own, tok.shape[2])
        pre_act = jnp.dot(block, weights(), preferred_element_type=jnp.float32)
        kept = jnp.square(jnp.maximum(pre_act, 0.0)).astype(jnp.bfloat16)
        hidden[pl.ds(pl.multiple_of(n * chunk * own, chunk * own), chunk * own), :] = kept

    def half_product(side, piece):
        picked = hidden[pl.ds(pl.multiple_of(side * rows, rows), rows), :]
        product = jnp.dot(picked, down[piece], preferred_element_type=jnp.float32)
        return product.reshape(pairs, own, Dc)

    def project(piece):
        s1[piece] = half_product(1 - c, piece).astype(jnp.bfloat16)
        swap = remote(s1.at[piece], r1.at[piece], s1_send.at[piece], r1_recv.at[piece], partner)
        swap.start()
        acc[...] = half_product(c, piece)
        swap.wait_recv()
        for k, (device, target, _) in enumerate(peers):
            s2[piece, k] = (acc[target] + r1[piece, target].astype(jnp.float32)).astype(jnp.bfloat16)
            remote(s2.at[piece, k], r2.at[piece, k], s2_send.at[piece], r2_recv.at[piece], device).start()
        own2[piece] = acc[q] + r1[piece, q].astype(jnp.float32)

    def visit(v):
        s = (v - 1) // 2
        odd = v % 2 == 1
        piece = jnp.where(v == 0, f, jnp.where(odd, f - 1 - s, f + 1 + s))
        to = jnp.where(odd, f + 1, f - 1)
        here = jnp.logical_and(piece >= 0, piece < F)
        onward = jnp.logical_and(jnp.logical_and(here, v > 0), jnp.logical_and(to >= 0, to < F))
        return piece, to, here, onward

    @pl.loop(0, last + 1)
    def _(v):
        piece, to, here, onward = visit(v)

        @pl.when(jnp.logical_and(here, v > 0))
        def _():
            for part in range(2):
                down_copy(piece, part, f, v).wait_recv()

                @pl.when(onward)
                def _():
                    down_copy(piece, part, to, v).start()

        @pl.when(here)
        def _():
            project(piece)

    for piece in range(F):
        pltpu.make_async_copy(r2.at[piece], r2.at[piece], r2_recv.at[piece]).wait()

    summed = []
    for piece in range(F):
        part = residual_scale * tok[mine, :, piece * Dc:(piece + 1) * Dc].astype(jnp.float32) + own2[piece]
        for k in range(len(peers)):
            part = part + r2[piece, k].astype(jnp.float32)
        summed.append(part)
    width = F * Dc
    row_mean = functools.reduce(jnp.add, [jnp.sum(p, axis=-1, keepdims=True) for p in summed]) / width
    centered = [p - row_mean for p in summed]
    row_var = functools.reduce(jnp.add, [jnp.sum(p * p, axis=-1, keepdims=True) for p in centered]) / width
    inverse = lax.rsqrt(row_var + norm_eps)
    for piece in range(F):
        cols = slice(piece * Dc, (piece + 1) * Dc)
        out_ref[:, cols] = (centered[piece] * inverse * gain_ref[:, cols] + shift_ref[:, cols]).astype(out_ref.dtype)

    own_sends_done = lambda copy: (
        guarded(f < F - 1, lambda: copy(f + 1, last + 1).wait_send()),
        guarded(f > 0, lambda: copy(f - 1, 0).wait_send()),
    )
    own_sends_done(lambda to, n: up_copy(f, to, n))
    for part in range(2):
        own_sends_done(lambda to, n: down_copy(f, part, to, n))
    for copy in tok_copies + fwd_copies:
        copy.wait_send()
    for v in range(1, last + 1):
        piece, to, here, onward = up_visit(v)
        guarded(onward, lambda: up_copy(piece, to, v).wait_send())
        for part in range(2):
            guarded(onward, lambda: down_copy(piece, part, to, v).wait_send())
    for piece in range(F):
        remote(s1.at[piece], r1.at[piece], s1_send.at[piece], r1_recv.at[piece], partner).wait_send()
        pltpu.make_async_copy(s2.at[piece], s2.at[piece], s2_send.at[piece]).wait()


def shards(sizes, tokens, w_up, w_down, out_gain, out_shift):
    R, F, T = sizes
    pairs = R * T // 2
    group = R * T
    own, D = tokens.shape
    H = w_up.shape[1] // R
    Dc = w_down.shape[1]
    others = pairs - 1
    visits = 2 * F
    dma = pltpu.SemaphoreType.DMA
    whole = pl.BlockSpec(memory_space=pltpu.VMEM)
    anywhere = pl.BlockSpec(memory_space=pl.ANY)
    return pl.pallas_call(
        functools.partial(kernel, sizes),
        out_shape=jax.ShapeDtypeStruct((own, D), jnp.bfloat16),
        in_specs=[anywhere, anywhere, anywhere, whole, whole],
        out_specs=whole,
        scratch_shapes=[
            pltpu.VMEM((group, own, D), jnp.bfloat16),
            pltpu.VMEM((F, D // F, H), jnp.bfloat16),
            pltpu.VMEM((F, H, Dc), jnp.bfloat16),
            pltpu.VMEM((group * own, H), jnp.bfloat16),
            pltpu.VMEM((F, pairs, own, Dc), jnp.bfloat16),
            pltpu.VMEM((F, pairs, own, Dc), jnp.bfloat16),
            pltpu.VMEM((pairs, own, Dc), jnp.float32),
            pltpu.VMEM((F, others, own, Dc), jnp.bfloat16),
            pltpu.VMEM((F, others, own, Dc), jnp.bfloat16),
            pltpu.VMEM((F, own, Dc), jnp.float32),
            dma((3,)),
            dma((pairs,)),
            dma((group,)),
            dma((others,)),
            dma((visits,)),
            dma((F,)),
            dma((visits, 2)),
            dma((F, 2)),
            dma((F,)),
            dma((F,)),
            dma((F,)),
            dma((F,)),
        ],
        compiler_params=pltpu.CompilerParams(
            collective_id=0, has_side_effects=True, vmem_limit_bytes=48 * 1024 * 1024
        ),
        name="feed_forward",
    )(tokens, w_up, w_down, out_gain.reshape(1, D), out_shift.reshape(1, D))


def solution(mesh):
    sizes = (mesh.shape["rep"], mesh.shape["fs"], mesh.shape["tp"])
    in_specs = (P(("rep", "fs", "tp"), None), P("fs", "tp"), P("tp", "fs"), P(), P())
    out_specs = P(("rep", "fs", "tp"), None)
    return jax.shard_map(
        functools.partial(shards, sizes), mesh=mesh, in_specs=in_specs, out_specs=out_specs, check_vma=False
    )
```

time: 163 us -> 52.6 us (0.32)
  waiting for transfers between devices: 140 us -> 0 us
  Pallas kernels: 0 us -> 47.2 us
  between operations: 13.2 us -> 0.01 us
  matrix products: 5.85 us -> 0 us
  local copies, waits for them, and re-layouts: 0.01 us -> 5.11 us
  other arithmetic: 4.1 us -> 0 us
    all_gather x3 -> x0, waiting for transfers between devices: 114 us -> none  [the longest x1 47.9 us: shards(): down_block = lax.all_gather(w_down, 'fs', axis=1, tiled=True)]
    pallas_call x0 -> x1, Pallas kernels: none -> 47.2 us  [shards(): pl.pallas_call(functools.partial(kernel, sizes), out_shape=jax.ShapeDtype...]
    reduce_scatter x1 -> x0, waiting for transfers between devices: 23.3 us -> none  [summed_rows(): lax.psum_scatter(whole, axis, scatter_dimension=0, tiled=True)]
    dot_general x1 -> x0, matrix products: 5.85 us -> none  [project(): return jnp.dot(picked, down_block, preferred_element_type=jnp.float32)]
    unnamed x6 -> x11, local copies, waits for them, and re-layouts: 0.01 us -> 5.11 us
    reduce_sum x2 -> x0, other arithmetic: 2.27 us -> none  [the longest x1 1.15 us: layer_norm(): row_var = jnp.mean(centered * centered, axis=-1, keepdims=True)]
    unnamed x4 -> x0, waiting for transfers between devices: 2.1 us -> none
    convert_element_type x1 -> x0, other arithmetic: 1.81 us -> none  [shards(): return layer_norm(summed, out_gain, out_shift).astype(jnp.bfloat16)]
  transfers between devices with their start and end apart: 4 -> 0, of which waited for: 4 -> 0; matrix products, arithmetic and copies ran while one was open for 0% -> 0% of each run, Pallas kernels for 0% -> 0%
where the time goes in v1:
time: 52.6 us; the launch traced here: 52.3 us
  Pallas kernels  47.2 us (90%)
  local copies, waits for them, and re-layouts  5.11 us (10%)
    pallas_call x1, Pallas kernels, shards(): pl.pallas_call(functools.partial(kernel, sizes), out_shape=jax.ShapeDtype...  47.2 us
    unnamed x11, local copies, waits for them, and re-layouts  5.11 us

profile of v1, /device:TPU:0, one launch (start us, length us, event | category | flops | bytes accessed | tf_op | source)
XLA Modules:
  0.0 52.3 jit_solution(8623701901985479274)
XLA Ops:
  0.0 0.0 copy-start
  0.0 1.0 %copy-done = bf16[256,1024]{1,0:T(8,128)(2,1)S(1)} copy-done((bf16[256,1024]{1,0:T(8,128)(2,1)S(1)}, bf16[256,1024]{1,0:T(8,128)(2,1)}, u32[]{:S(2)}) %copy-start) | copy-done | bytes 524312
  1.0 0.0 copy-start.1
  1.0 1.0 %copy-done.1 = bf16[1024,256]{1,0:T(8,128)(2,1)S(1)} copy-done((bf16[1024,256]{1,0:T(8,128)(2,1)S(1)}, bf16[1024,256]{1,0:T(8,128)(2,1)}, u32[]{:S(2)}) %copy-start.1) | copy-done | bytes 524312
  2.1 0.0 copy-start.2
  2.1 0.9 %copy-done.2 = bf16[128,1024]{1,0:T(8,128)(2,1)S(1)} copy-done((bf16[128,1024]{1,0:T(8,128)(2,1)S(1)}, bf16[128,1024]{1,0:T(8,128)(2,1)}, u32[]{:S(2)}) %copy-start.2) | copy-done | bytes 262168
  3.0 0.0 copy-start.3
  3.0 0.7 %copy-done.3 = f32[1024]{0:T(1024)S(1)} copy-done((f32[1024]{0:T(1024)S(1)}, f32[1024]{0:T(1024)}, u32[]{:S(2)}) %copy-start.3) | copy-done | bytes 4120
  3.7 0.0 copy-start.4
  3.7 0.7 %copy-done.4 = f32[1024]{0:T(1024)S(1)} copy-done((f32[1024]{0:T(1024)S(1)}, f32[1024]{0:T(1024)}, u32[]{:S(2)}) %copy-start.4) | copy-done | bytes 4120
  4.4 47.2 %feed_forward.1 = bf16[128,1024]{1,0:T(8,128)(2,1)S(1)} custom-call(bf16[128,1024]{1,0:T(8,128)(2,1)S(1)} %copy-done.2, bf16[256,1024]{1,0:T(8,128)(2,1)S(1)} %copy-done, bf16[1024,256]{1,0:T(8,128)(2,1)S(1)} %copy-done.1, f32[1,1024]{1,0:T(1,128)S(1)} %bitcast.2, f32[1,1024]{1,0:T(1,128)S(1)} %bitcast.3), custom_call_target="tpu_custom_call" | custom-call | tf_op jit(solution)/shard_map/feed_forward/pallas_call | solution.py:246
  51.6 0.7 %copy.7 = bf16[128,1024]{1,0:T(8,128)(2,1)} copy(bf16[128,1024]{1,0:T(8,128)(2,1)S(1)} %feed_forward.1) | data formatting | bytes 524288
Async XLA Ops:
  0.0 1.0 %copy-start = (bf16[256,1024]{1,0:T(8,128)(2,1)S(1)}, bf16[256,1024]{1,0:T(8,128)(2,1)}, u32[]{:S(2)}) copy-start(bf16[256,1024]{1,0:T(8,128)(2,1)} %up_ref.1) | copy-start | bytes 1572868
  1.0 1.0 %copy-start.1 = (bf16[1024,256]{1,0:T(8,128)(2,1)S(1)}, bf16[1024,256]{1,0:T(8,128)(2,1)}, u32[]{:S(2)}) copy-start(bf16[1024,256]{1,0:T(8,128)(2,1)} %down_ref.1) | copy-start | bytes 1572868
  2.1 0.9 %copy-start.2 = (bf16[128,1024]{1,0:T(8,128)(2,1)S(1)}, bf16[128,1024]{1,0:T(8,128)(2,1)}, u32[]{:S(2)}) copy-start(bf16[128,1024]{1,0:T(8,128)(2,1)} %tokens_ref.1) | copy-start | bytes 786436
  3.0 0.7 %copy-start.3 = (f32[1024]{0:T(1024)S(1)}, f32[1024]{0:T(1024)}, u32[]{:S(2)}) copy-start(f32[1024]{0:T(1024)} %param.8) | copy-start | bytes 12292
  3.7 0.7 %copy-start.4 = (f32[1024]{0:T(1024)S(1)}, f32[1024]{0:T(1024)}, u32[]{:S(2)}) copy-start(f32[1024]{0:T(1024)} %param.9) | copy-start | bytes 12292

commit v2 on v1

v2 whole, which is shorter than its diff:
```python
import functools

import jax
import jax.numpy as jnp
from jax import lax
from jax.experimental import pallas as pl
from jax.experimental.pallas import tpu as pltpu
from jax.sharding import PartitionSpec as P

residual_scale = 2.0**0.25
norm_eps = 1e-05


def kernel(
    sizes,
    tokens_ref, up_ref, down_ref, gain_ref, shift_ref,
    out_ref,
    tok, up, down, gain, shift, hidden, s1, r1, acc, s2, r2, own2,
    load_sem, tok_send, tok_recv, fwd_send, up_send, up_recv,
    down_send, down_recv, s1_send, r1_recv, s2_send, r2_recv,
):
    R, F, T = sizes
    Y = T // 2
    pairs = R * Y
    own = tokens_ref.shape[0]
    H = up.shape[2]
    parts = down.shape[0] // F
    Dp = down.shape[2]
    r, f, t = lax.axis_index("rep"), lax.axis_index("fs"), lax.axis_index("tp")
    y, c = t // 2, t % 2
    q = r * Y + y
    mine = c * pairs + q

    def dev(rr, ff, tt):
        return {"rep": rr, "fs": ff, "tp": tt}

    partner = dev(r, f, y * 2 + (1 - c))
    peers = []
    for dr in range(R):
        for dy in range(Y):
            if dr or dy:
                rr, yy = (r + dr) % R, (y + dy) % Y
                sr, sy = (r + R - dr) % R, (y + Y - dy) % Y
                peers.append((dev(rr, f, yy * 2 + c), rr * Y + yy, sr * Y + sy))

    def remote(src, dst, ss, rs, device):
        return pltpu.make_async_remote_copy(
            src_ref=src, dst_ref=dst, send_sem=ss, recv_sem=rs,
            device_id=device, device_id_type=pl.DeviceIdType.MESH,
        )

    base = pl.multiple_of(r * H, H)
    loads = [
        pltpu.make_async_copy(up_ref.at[:, pl.ds(base, H)], up.at[f], load_sem.at[0]),
        pltpu.make_async_copy(tokens_ref, tok.at[mine], load_sem.at[1]),
        pltpu.make_async_copy(gain_ref, gain, load_sem.at[2]),
        pltpu.make_async_copy(shift_ref, shift, load_sem.at[3]),
    ]
    for part in range(parts):
        block = down_ref.at[pl.ds(base, H), pl.ds(part * Dp, Dp)]
        loads.append(pltpu.make_async_copy(block, down.at[f * parts + part], load_sem.at[4 + part]))
    for load in loads:
        load.start()

    barrier = pltpu.get_barrier_semaphore()

    def greet(device):
        pl.semaphore_signal(barrier, inc=1, device_id=device, device_id_type=pl.DeviceIdType.MESH)

    greet(partner)
    for device, _, _ in peers:
        greet(device)

    @pl.when(f > 0)
    def _():
        greet(dev(r, f - 1, t))

    @pl.when(f < F - 1)
    def _():
        greet(dev(r, f + 1, t))

    neighbours = jnp.where(f > 0, 1, 0) + jnp.where(f < F - 1, 1, 0)
    pl.semaphore_wait(barrier, 1 + len(peers) + neighbours)

    def up_copy(piece, to, n):
        return remote(up.at[piece], up.at[piece], up_send.at[n], up_recv.at[piece], dev(r, to, t))

    def down_copy(piece, part, to, n):
        block = down.at[piece * parts + part]
        return remote(block, block, down_send.at[n, part], down_recv.at[piece, part], dev(r, to, t))

    def guarded(condition, action):
        @pl.when(condition)
        def _():
            action()

    last = 2 * F - 2

    def own_sends(copy):
        guarded(f < F - 1, lambda: copy(f + 1, last + 1).start())
        guarded(f > 0, lambda: copy(f - 1, 0).start())

    loads[0].wait()
    own_sends(lambda to, n: up_copy(f, to, n))
    loads[1].wait()
    tok_copies = [remote(tok.at[mine], tok.at[mine], tok_send.at[0], tok_recv.at[mine], partner)]
    for k, (device, _, _) in enumerate(peers):
        tok_copies.append(remote(tok.at[mine], tok.at[mine], tok_send.at[k + 1], tok_recv.at[mine], device))
    for copy in tok_copies[1:] + tok_copies[:1]:
        copy.start()
    for load in loads[2:]:
        load.wait()
    own_sends(lambda to, n: down_copy(f, 0, to, n))

    def up_visit(v):
        s = (v - 1) // 2
        if v % 2:
            piece, to = f - 1 - s, f + 1
            here, onward = piece >= 0, jnp.logical_and(piece >= 0, f < F - 1)
        else:
            piece, to = f + 1 + s, f - 1
            here, onward = piece < F, jnp.logical_and(piece < F, f > 0)
        return piece, to, here, onward

    def take_up(v):
        piece, to, here, onward = up_visit(v)
        guarded(here, lambda: up_copy(piece, f, v).wait_recv())
        guarded(onward, lambda: up_copy(piece, to, v).start())

    for v in (1, 2):
        if v <= last:
            take_up(v)
    for part in range(1, parts):
        own_sends(lambda to, n: down_copy(f, part, to, n))

    fwd_copies = []
    for k, (_, _, source) in enumerate(peers):
        slot = c * pairs + source
        remote(tok.at[slot], tok.at[slot], tok_send.at[0], tok_recv.at[slot], partner).wait_recv()
        fwd = remote(tok.at[slot], tok.at[slot], fwd_send.at[k], tok_recv.at[slot], partner)
        fwd.start()
        fwd_copies.append(fwd)

    for v in range(3, last + 1):
        take_up(v)
    for k in range(pairs):
        slot = (1 - c) * pairs + k
        remote(tok.at[slot], tok.at[slot], tok_send.at[0], tok_recv.at[slot], partner).wait_recv()

    def visit(v):
        step = (v - 1) // 2
        odd = v % 2 == 1
        piece = jnp.where(odd, f - 1 - step, f + 1 + step)
        to = jnp.where(odd, f + 1, f - 1)
        here = jnp.logical_and(v <= last, jnp.logical_and(piece >= 0, piece < F))
        passes = jnp.logical_and(to >= 0, to < F)
        return piece, to, jnp.logical_and(here, passes), jnp.logical_and(here, jnp.logical_not(passes))

    def pass_down(v):
        piece, to, onward, _ = visit(v)

        @pl.when(onward)
        def _():
            for part in range(parts):
                down_copy(piece, part, f, v).wait_recv()
                down_copy(piece, part, to, v).start()

    for v in (1, 2):
        if v <= last:
            pass_down(v)

    rows = pairs * own
    chunk = 2 if pairs % 2 == 0 else 1
    weights = lambda: up[...].reshape(up.shape[0] * up.shape[1], H)

    @pl.loop(0, 2 * pairs // chunk)
    def _(n):
        block = tok[pl.ds(n * chunk, chunk)].reshape(chunk * own, tok.shape[2])
        pre_act = jnp.dot(block, weights(), preferred_element_type=jnp.float32)
        kept = jnp.square(jnp.maximum(pre_act, 0.0)).astype(jnp.bfloat16)
        hidden[pl.ds(pl.multiple_of(n * chunk * own, chunk * own), chunk * own), :] = kept

    def half_product(side, block):
        picked = hidden[pl.ds(pl.multiple_of(side * rows, rows), rows), :]
        product = jnp.dot(picked, down[block], preferred_element_type=jnp.float32)
        return product.reshape(pairs, own, Dp)

    def project(block):
        s1[block] = half_product(1 - c, block).astype(jnp.bfloat16)
        swap = remote(s1.at[block], r1.at[block], s1_send.at[block], r1_recv.at[block], partner)
        swap.start()
        acc[...] = half_product(c, block)
        swap.wait_recv()
        for k, (device, target, _) in enumerate(peers):
            s2[block, k] = (acc[target] + r1[block, target].astype(jnp.float32)).astype(jnp.bfloat16)
            remote(s2.at[block, k], r2.at[block, k], s2_send.at[block], r2_recv.at[block], device).start()
        own2[block] = acc[q] + r1[block, q].astype(jnp.float32)

    @pl.loop(0, F)
    def _(step):
        @pl.when(step > 0)
        def _():
            pass_down(2 * step + 1)
            pass_down(2 * step + 2)

        @pl.loop(0, 2 * parts)
        def _(n):
            part = n % parts
            v = 2 * step - 1 + n // parts
            piece, _, onward, ends = visit(v)
            piece = jnp.where(step == 0, f, piece)
            remote_here = jnp.logical_and(step > 0, jnp.logical_or(onward, ends))

            @pl.when(jnp.logical_and(step > 0, ends))
            def _():
                down_copy(piece, part, f, 0).wait_recv()

            @pl.when(jnp.logical_or(remote_here, jnp.logical_and(step == 0, n < parts)))
            def _():
                project(piece * parts + part)

    blocks = F * parts
    for block in range(blocks):
        pltpu.make_async_copy(r2.at[block], r2.at[block], r2_recv.at[block]).wait()

    summed = []
    for block in range(blocks):
        term = residual_scale * tok[mine, :, block * Dp:(block + 1) * Dp].astype(jnp.float32) + own2[block]
        for k in range(len(peers)):
            term = term + r2[block, k].astype(jnp.float32)
        summed.append(term)
    width = blocks * Dp
    row_mean = functools.reduce(jnp.add, [jnp.sum(p, axis=-1, keepdims=True) for p in summed]) / width
    centered = [p - row_mean for p in summed]
    row_var = functools.reduce(jnp.add, [jnp.sum(p * p, axis=-1, keepdims=True) for p in centered]) / width
    inverse = lax.rsqrt(row_var + norm_eps)
    for block in range(blocks):
        cols = slice(block * Dp, (block + 1) * Dp)
        out_ref[:, cols] = (centered[block] * inverse * gain[:, cols] + shift[:, cols]).astype(out_ref.dtype)

    own_sends_done = lambda copy: (
        guarded(f < F - 1, lambda: copy(f + 1, last + 1).wait_send()),
        guarded(f > 0, lambda: copy(f - 1, 0).wait_send()),
    )
    own_sends_done(lambda to, n: up_copy(f, to, n))
    for part in range(parts):
        own_sends_done(lambda to, n: down_copy(f, part, to, n))
    for copy in tok_copies + fwd_copies:
        copy.wait_send()
    for v in range(1, last + 1):
        piece, to, here, onward = up_visit(v)
        guarded(onward, lambda: up_copy(piece, to, v).wait_send())
        for part in range(parts):
            guarded(onward, lambda: down_copy(piece, part, to, v).wait_send())
    for block in range(blocks):
        remote(s1.at[block], r1.at[block], s1_send.at[block], r1_recv.at[block], partner).wait_send()
        pltpu.make_async_copy(s2.at[block], s2.at[block], s2_send.at[block]).wait()


def shards(sizes, tokens, w_up, w_down, out_gain, out_shift):
    R, F, T = sizes
    pairs = R * T // 2
    group = R * T
    own, D = tokens.shape
    H = w_up.shape[1] // R
    Dc = w_down.shape[1]
    others = pairs - 1
    visits = 2 * F
    parts = 2 if Dc % 256 == 0 else 1
    blocks, Dp = F * parts, Dc // parts
    dma = pltpu.SemaphoreType.DMA
    whole = pl.BlockSpec(memory_space=pltpu.VMEM)
    in_hbm = pl.BlockSpec(memory_space=pltpu.HBM)
    return pl.pallas_call(
        functools.partial(kernel, sizes),
        out_shape=jax.ShapeDtypeStruct((own, D), jnp.bfloat16),
        in_specs=[in_hbm] * 5,
        out_specs=whole,
        scratch_shapes=[
            pltpu.VMEM((group, own, D), jnp.bfloat16),
            pltpu.VMEM((F, D // F, H), jnp.bfloat16),
            pltpu.VMEM((blocks, H, Dp), jnp.bfloat16),
            pltpu.VMEM((1, D), jnp.float32),
            pltpu.VMEM((1, D), jnp.float32),
            pltpu.VMEM((group * own, H), jnp.bfloat16),
            pltpu.VMEM((blocks, pairs, own, Dp), jnp.bfloat16),
            pltpu.VMEM((blocks, pairs, own, Dp), jnp.bfloat16),
            pltpu.VMEM((pairs, own, Dp), jnp.float32),
            pltpu.VMEM((blocks, others, own, Dp), jnp.bfloat16),
            pltpu.VMEM((blocks, others, own, Dp), jnp.bfloat16),
            pltpu.VMEM((blocks, own, Dp), jnp.float32),
            dma((4 + parts,)),
            dma((pairs,)),
            dma((group,)),
            dma((others,)),
            dma((visits,)),
            dma((F,)),
            dma((visits, parts)),
            dma((F, parts)),
            dma((blocks,)),
            dma((blocks,)),
            dma((blocks,)),
            dma((blocks,)),
        ],
        compiler_params=pltpu.CompilerParams(
            collective_id=0, has_side_effects=True, vmem_limit_bytes=67_043_328
        ),
        name="feed_forward",
    )(tokens, w_up, w_down, out_gain.reshape(1, D), out_shift.reshape(1, D))


def solution(mesh):
    sizes = (mesh.shape["rep"], mesh.shape["fs"], mesh.shape["tp"])
    in_specs = (P(("rep", "fs", "tp"), None), P("fs", "tp"), P("tp", "fs"), P(), P())
    out_specs = P(("rep", "fs", "tp"), None)
    return jax.shard_map(
        functools.partial(shards, sizes), mesh=mesh, in_specs=in_specs, out_specs=out_specs, check_vma=False
    )
```

time: 52.6 us -> 52.5 us (level)
  local copies, waits for them, and re-layouts: 5.11 us -> 1.67 us
  Pallas kernels: 47.2 us -> 50.6 us
    unnamed x11 -> x1, local copies, waits for them, and re-layouts: 5.11 us -> 1.67 us
    pallas_call x1, Pallas kernels: 47.2 us -> 50.6 us  [shards(): pl.pallas_call(functools.partial(kernel, sizes), out_shape=jax.ShapeDtype...]
where the time goes in v2:
time: 52.5 us; the launch traced here: 52.3 us
  Pallas kernels  50.6 us (96%)
  local copies, waits for them, and re-layouts  1.67 us (3%)
    pallas_call x1, Pallas kernels, shards(): pl.pallas_call(functools.partial(kernel, sizes), out_shape=jax.ShapeDtype...  50.6 us
    unnamed x1, local copies, waits for them, and re-layouts  1.67 us

profile of v2, /device:TPU:0, one launch (start us, length us, event | category | flops | bytes accessed | tf_op | source)
XLA Modules:
  0.0 52.3 jit_solution(18065228335633919048)
XLA Ops:
  0.0 50.6 %feed_forward.1 = bf16[128,1024]{1,0:T(8,128)(2,1)} custom-call(bf16[128,1024]{1,0:T(8,128)(2,1)} %tokens_ref.1, bf16[256,1024]{1,0:T(8,128)(2,1)} %up_ref.1, bf16[1024,256]{1,0:T(8,128)(2,1)} %down_ref.1, f32[1,1024]{1,0:T(1,128)} %bitcast.2, f32[1,1024]{1,0:T(1,128)} %bitcast.3), custom_call_target="tpu_custom_call" | custom-call | tf_op jit(solution)/shard_map/feed_forward/pallas_call | solution.py:274
  50.6 1.7 %copy.7 = bf16[128,1024]{1,0:T(8,128)(2,1)} copy(bf16[128,1024]{1,0:T(8,128)(2,1)} %feed_forward.1) | data formatting | bytes 524288

commit v3 on v2

--- a/solution.py
+++ b/solution.py
@@ -133,20 +133,6 @@
     for part in range(1, parts):
         own_sends(lambda to, n: down_copy(f, part, to, n))
 
-    fwd_copies = []
-    for k, (_, _, source) in enumerate(peers):
-        slot = c * pairs + source
-        remote(tok.at[slot], tok.at[slot], tok_send.at[0], tok_recv.at[slot], partner).wait_recv()
-        fwd = remote(tok.at[slot], tok.at[slot], fwd_send.at[k], tok_recv.at[slot], partner)
-        fwd.start()
-        fwd_copies.append(fwd)
-
-    for v in range(3, last + 1):
-        take_up(v)
-    for k in range(pairs):
-        slot = (1 - c) * pairs + k
-        remote(tok.at[slot], tok.at[slot], tok_send.at[0], tok_recv.at[slot], partner).wait_recv()
-
     def visit(v):
         step = (v - 1) // 2
         odd = v % 2 == 1
@@ -156,8 +142,10 @@
         passes = jnp.logical_and(to >= 0, to < F)
         return piece, to, jnp.logical_and(here, passes), jnp.logical_and(here, jnp.logical_not(passes))
 
-    def pass_down(v):
+    def pass_down(v, only=None):
         piece, to, onward, _ = visit(v)
+        if only is not None:
+            onward = jnp.logical_and(onward, only(piece))
 
         @pl.when(onward)
         def _():
@@ -165,9 +153,30 @@
                 down_copy(piece, part, f, v).wait_recv()
                 down_copy(piece, part, to, v).start()
 
+    def from_end(piece):
+        return jnp.logical_or(piece == 0, piece == F - 1)
+
     for v in (1, 2):
         if v <= last:
-            pass_down(v)
+            pass_down(v, from_end)
+
+    fwd_copies = []
+    for k, (_, _, source) in enumerate(peers):
+        slot = c * pairs + source
+        remote(tok.at[slot], tok.at[slot], tok_send.at[0], tok_recv.at[slot], partner).wait_recv()
+        fwd = remote(tok.at[slot], tok.at[slot], fwd_send.at[k], tok_recv.at[slot], partner)
+        fwd.start()
+        fwd_copies.append(fwd)
+
+    for v in range(3, last + 1):
+        take_up(v)
+    for k in range(pairs):
+        slot = (1 - c) * pairs + k
+        remote(tok.at[slot], tok.at[slot], tok_send.at[0], tok_recv.at[slot], partner).wait_recv()
+
+    for v in (1, 2):
+        if v <= last:
+            pass_down(v, lambda piece: jnp.logical_not(from_end(piece)))
 
     rows = pairs * own
     chunk = 2 if pairs % 2 == 0 else 1
@@ -198,10 +207,8 @@
 
     @pl.loop(0, F)
     def _(step):
-        @pl.when(step > 0)
-        def _():
-            pass_down(2 * step + 1)
-            pass_down(2 * step + 2)
+        pass_down(2 * step + 3)
+        pass_down(2 * step + 4)
 
         @pl.loop(0, 2 * parts)
         def _(n):
@@ -303,7 +310,7 @@
             dma((blocks,)),
         ],
         compiler_params=pltpu.CompilerParams(
-            collective_id=0, has_side_effects=True, vmem_limit_bytes=67_043_328
+            collective_id=0, has_side_effects=True, vmem_limit_bytes=67_043_328 - 2 * 8 * D - 2 * own * D
         ),
         name="feed_forward",
     )(tokens, w_up, w_down, out_gain.reshape(1, D), out_shift.reshape(1, D))

time: 52.5 us -> 52.5 us (level)
  no operation moved by 1% of the time
where the time goes in v3:
time: 52.5 us; the launch traced here: 52.4 us
  Pallas kernels  50.7 us (97%)
  local copies, waits for them, and re-layouts  1.67 us (3%)
    pallas_call x1, Pallas kernels, shards(): pl.pallas_call(functools.partial(kernel, sizes), out_shape=jax.ShapeDtype...  50.7 us
    unnamed x1, local copies, waits for them, and re-layouts  1.67 us

profile of v3, /device:TPU:0, one launch (start us, length us, event | category | flops | bytes accessed | tf_op | source)
XLA Modules:
  0.0 52.4 jit_solution(10065390410582368253)
XLA Ops:
  0.0 50.7 %feed_forward.1 = bf16[128,1024]{1,0:T(8,128)(2,1)} custom-call(bf16[128,1024]{1,0:T(8,128)(2,1)} %tokens_ref.1, bf16[256,1024]{1,0:T(8,128)(2,1)} %up_ref.1, bf16[1024,256]{1,0:T(8,128)(2,1)} %down_ref.1, f32[1,1024]{1,0:T(1,128)} %bitcast.2, f32[1,1024]{1,0:T(1,128)} %bitcast.3), custom_call_target="tpu_custom_call" | custom-call | tf_op jit(solution)/shard_map/feed_forward/pallas_call | solution.py:281
  50.7 1.7 %copy.7 = bf16[128,1024]{1,0:T(8,128)(2,1)} copy(bf16[128,1024]{1,0:T(8,128)(2,1)} %feed_forward.1) | data formatting | bytes 524288
